TPU v7x, 32 devices: a whole 2x2x4 slice. The times are simulated.
32 devices in a mesh: gr: 2 (over y), fs: 4 (over z), tp: 4 (over x, core).
Axes of the slice: x: 2, y: 2, z: 4, core: 2. Of those that a mesh axis runs over, the one named last changes fastest.
Arguments:
- prompt: bfloat16 [4096, 2048], P(('gr', 'fs')), may hold values from -6 to 6
- norm_gain: float32 [2048], P(('gr', 'fs')), may hold values from 0.1 to 1.9
- gate_master: float32 [32, 2048, 1024], P(None, ('gr', 'fs'), 'tp'), may hold values from -6 to 6
- up_master: float32 [32, 2048, 1024], P(None, ('gr', 'fs'), 'tp'), may hold values from -6 to 6
- down_master: float32 [32, 2048, 1024], P(None, ('gr', 'fs'), 'tp'), may hold values from -6 to 6
- routes: int32 [4096, 2], P(('gr', 'fs')), may hold values from 0 to 31, as said below
- route_weights: float32 [4096, 2], P(('gr', 'fs')), may hold values from 0.1 to 0.9
Outputs:
- gate_ready: bfloat16 [32, 2048, 1024], P('fs', None, 'tp')
- up_ready: bfloat16 [32, 2048, 1024], P('fs', None, 'tp')
- down_ready: bfloat16 [32, 2048, 1024], P('fs', None, 'tp')
- blended: bfloat16 [4096, 2048], P(('gr', 'fs'), 'tp')
Inputs may be any that keep to these rules, and one draw needn't show every extreme that they name: `routes`: each row names 2 different experts of one group: expert // 8 is the group. In every aligned block of 512 rows (the tokens of one index of gr and fs) half of the rows choose one group, and no expert is named more than 64 times; in every block some expert is named exactly 64 times.
All inputs are finite; a program needn't handle non-finite values.
Results may differ from a plain program's by a relative error of at most 0.015.
Values may be sent and summed in bfloat16 or wider, within the bound.
A program may use at most 128 MiB of HBM per device.

v0:
```python
import jax
import jax.numpy as jnp
from jax import lax
from jax.sharding import PartitionSpec as P

D = 2048
FF = 1024
EPS = 1e-06


def per_device(prompt, norm_gain, gate_master, up_master, down_master, routes, route_weights):
    gate_low = (norm_gain[None, :, None] * gate_master).astype(jnp.bfloat16)
    up_low = (norm_gain[None, :, None] * up_master).astype(jnp.bfloat16)
    down_low = down_master.astype(jnp.bfloat16)
    experts = gate_low.shape[0]
    fs_count = lax.axis_size("fs")
    local_experts = experts // fs_count
    resharded = (
        lax.all_to_all(gate_low, "fs", split_axis=0, concat_axis=1, tiled=True),
        lax.all_to_all(up_low, "fs", split_axis=0, concat_axis=1, tiled=True),
        lax.all_to_all(down_low, "fs", split_axis=0, concat_axis=1, tiled=True),
    )
    gate_ready, up_ready, down_ready = (
        lax.all_gather(resharded[0], "gr", axis=1, tiled=True),
        lax.all_gather(resharded[1], "gr", axis=1, tiled=True),
        lax.all_gather(resharded[2], "gr", axis=1, tiled=True),
    )
    tokens = prompt.shape[0]
    capacity = tokens // 8
    prompt_wide = prompt.astype(jnp.float32)
    normed = (
        prompt_wide * lax.rsqrt(jnp.mean(prompt_wide * prompt_wide, axis=-1, keepdims=True) + EPS)
    ).astype(jnp.bfloat16)
    route_list = routes.reshape(-1)
    route_hits = (route_list[:, None] == jnp.arange(experts, dtype=jnp.int32)[None, :]).astype(
        jnp.int32
    )
    slot_rank = jnp.sum((jnp.cumsum(route_hits, axis=0) - 1) * route_hits, axis=1)
    slot_index = route_list * capacity + slot_rank
    token_of = jnp.arange(route_list.shape[0], dtype=jnp.int32) // routes.shape[1]
    slot_owner = jnp.zeros((experts * capacity,), jnp.int32).at[slot_index].set(token_of)
    outgoing = normed[slot_owner].reshape(fs_count, local_experts, capacity, normed.shape[1])
    arrived = lax.all_to_all(outgoing, "fs", split_axis=0, concat_axis=0, tiled=True)
    pre_gate = jnp.einsum(
        "secd,edf->secf", arrived, gate_ready, preferred_element_type=jnp.float32
    ) * D ** (-0.5)
    pre_up = jnp.einsum(
        "secd,edf->secf", arrived, up_ready, preferred_element_type=jnp.float32
    ) * D ** (-0.5)
    hidden = (jax.nn.silu(pre_gate) * pre_up).astype(jnp.bfloat16)
    partial_value = (
        jnp.einsum("secf,edf->secd", hidden, down_ready, preferred_element_type=jnp.float32)
        * FF ** (-0.5)
    ).astype(jnp.bfloat16)
    summed = lax.psum_scatter(partial_value, "tp", scatter_dimension=3, tiled=True).astype(
        jnp.float32
    )
    answers = lax.all_to_all(
        summed.astype(jnp.bfloat16), "fs", split_axis=0, concat_axis=0, tiled=True
    )
    answers_flat = answers.reshape(experts * capacity, answers.shape[3])
    picked = answers_flat[slot_index].reshape(tokens, routes.shape[1], answers.shape[3])
    blended = jnp.sum(picked.astype(jnp.float32) * route_weights[:, :, None], axis=1)
    return (gate_ready, up_ready, down_ready, blended.astype(jnp.bfloat16))


def solution(mesh):
    in_specs = (
        P(("gr", "fs"), None),
        P(("gr", "fs")),
        P(None, ("gr", "fs"), "tp"),
        P(None, ("gr", "fs"), "tp"),
        P(None, ("gr", "fs"), "tp"),
        P(("gr", "fs"), None),
        P(("gr", "fs"), None),
    )
    out_specs = (
        P("fs", None, "tp"),
        P("fs", None, "tp"),
        P("fs", None, "tp"),
        P(("gr", "fs"), "tp"),
    )
    return jax.shard_map(
        per_device, mesh=mesh, in_specs=in_specs, out_specs=out_specs, check_vma=False
    )
```

profile of v0, /device:TPU:0, one launch (start us, length us, event | category | flops | bytes accessed | tf_op | source)
XLA Modules:
  0.0 691.8 jit_solution(8240424116408428662)
XLA Ops:
  7.2 11.5 %multiply_convert_fusion.1 = (bf16[32,256,256]{2,1,0:T(8,128)(2,1)}, bf16[32,256,256]{2,1,0:T(8,128)(2,1)}) fusion(f32[32,256,256]{2,1,0:T(8,128)} %param.10, f32[256]{0:T(256)} %param.8, f32[32,256,256]{2,1,0:T(8,128)} %param.9), kind=kLoop, calls=%fused_computation.11 | loop fusion | flops 8388608 | bytes 25166848 | tf_op jit(solution)/shard_map/convert_element_type | solution.py:13
  18.7 100.6 %all_to_all.64 = bf16[32,256,256]{2,1,0:T(8,128)(2,1)} all-to-all(bf16[32,256,256]{2,1,0:T(8,128)(2,1)} %get-tuple-element.4), channel_id=1, replica_groups=mesh['gr'=2,'fs'=4,'tp'=4] {'fs'}, dimensions={0} | all-to-all | bytes 8388608 | tf_op jit(solution)/shard_map/all_to_all | solution.py:20
  119.2 4.9 all-to-all-start
  124.2 4.6 copy.27
  128.9 5.9 convert_element_type.42
  134.8 82.3 %all-to-all-done = bf16[32,256,256]{2,1,0:T(8,128)(2,1)} async-done(((bf16[32,256,256]{2,1,0:T(8,128)(2,1)}), bf16[32,256,256]{2,1,0:T(8,128)(2,1)}, u32[]{:S(2)}, u32[]{:S(2)}) %all-to-all-start) | async-done | bytes 4194336 | tf_op jit(solution)/shard_map/all_to_all | solution.py:19
  217.0 4.8 all-to-all-start.2
  221.9 4.6 copy.26
  226.6 0.7 copy-done.1
  227.8 9.0 %reduce-window.6 = s32[32,8,128]{2,1,0:T(8,128)S(1)} reduce-window(s32[32,8,128]{2,1,0:T(8,128)S(1)} %fusion.29, s32[]{:T(128)} %constant.36.clone.1), window={size=1x1x128 pad=0_0x0_0x127_0}, to_apply=%region_1.0 | reduce-window | flops 4161536 | bytes 262148 | tf_op jit(solution)/shard_map/reduce-window
  237.3 0.2 mul.86
  237.7 4.3 scatter_custom_fusion
  242.0 0.5 fusion.9
  242.5 2.3 fusion.10
  244.8 10.9 %gather_fusion = bf16[2048,2048]{1,0:T(8,128)(2,1)} fusion(bf16[512,2048]{1,0:T(8,128)(2,1)S(1)} %fusion.10, s32[2048]{0:T(1024)S(1)} %fusion.30), kind=kCustom, calls=%fused_computation | custom fusion | bytes 16785408 | tf_op jit(solution)/shard_map/gather | solution.py:42
  255.7 58.9 %all-to-all-done.2 = bf16[32,256,256]{2,1,0:T(8,128)(2,1)} async-done(((bf16[32,256,256]{2,1,0:T(8,128)(2,1)}), bf16[32,256,256]{2,1,0:T(8,128)(2,1)}, u32[]{:S(2)}, u32[]{:S(2)}) %all-to-all-start.2) | async-done | bytes 4194336 | tf_op jit(solution)/shard_map/all_to_all | solution.py:21
  314.6 5.7 all-to-all-start.3
  320.4 4.7 copy.28
  325.1 0.2 reduce-scatter.2.cloned.1.call-start
  325.3 177.6 %all-to-all-done.3 = bf16[4,8,64,2048]{3,2,1,0:T(8,128)(2,1)} async-done(((bf16[4,8,64,2048]{3,2,1,0:T(8,128)(2,1)}), bf16[4,8,64,2048]{3,2,1,0:T(8,128)(2,1)}, u32[]{:S(2)}, u32[]{:S(2)}) %all-to-all-start.3) | async-done | bytes 8388640 | tf_op jit(solution)/shard_map/all_to_all | solution.py:43
  502.9 8.1 %fusion.3 = f32[8,256,4,64]{1,3,2,0:T(8,128)S(1)} fusion(bf16[8,2048,256]{2,1,0:T(8,128)(2,1)} %all-gather.6.cloned.1.call-done, bf16[4,8,64,2048]{3,2,1,0:T(8,128)(2,1)} %all-to-all-done.3), kind=kOutput, calls=%fused_computation.7 | convolution fusion | flops 2147483648 | bytes 18874368 | tf_op jit(solution)/shard_map/secd,edf->secf/dot_general | solution.py:47
  511.1 17.0 %fusion = bf16[4,8,64,2048]{3,2,0,1:T(8,128)(2,1)} fusion(bf16[8,2048,256]{2,1,0:T(8,128)(2,1)} %all-gather.8.cloned.1.call-done, f32[8,256,4,64]{1,3,2,0:T(8,128)S(1)} %fusion.3, bf16[4,8,64,2048]{3,2,1,0:T(8,128)(2,1)} %all-to-all-done.3, bf16[8,2048,256]{2,1,0:T(8,128)(2,1)} %all-gather.4.cloned.1.call-done), kind=kOutput, calls=%fused_computation.4 | convolution fusion | flops 4307550208 | bytes 35651584 | tf_op jit(solution)/shard_map/secf,edf->secd/dot_general | solution.py:52
  528.2 70.0 %reduce-scatter.2.cloned.1.call-done = bf16[4,8,64,512]{3,2,0,1:T(8,128)(2,1)} async-done(((bf16[4,8,64,2048]{3,2,0,1:T(8,128)(2,1)}), bf16[4,8,64,512]{3,2,0,1:T(8,128)(2,1)}) %reduce-scatter.2.cloned.1.call-update) | async-done | bytes 2097168 | tf_op jit(solution)/shard_map/reduce_scatter | solution.py:55
  598.2 3.1 copy.36
  601.3 4.6 all-to-all-start.4
  606.1 47.9 %all-to-all-done.4 = bf16[4,8,64,512]{3,2,1,0:T(8,128)(2,1)S(1)} async-done(((bf16[4,8,64,512]{3,2,1,0:T(8,128)(2,1)}), bf16[4,8,64,512]{3,2,1,0:T(8,128)(2,1)S(1)}, u32[]{:S(2)}, u32[]{:S(2)}) %all-to-all-start.4) | async-done | bytes 2097184 | tf_op jit(solution)/shard_map/all_to_all | solution.py:58
  653.9 4.0 gather_fusion.1
  657.9 1.3 reshape.78
  659.3 4.0 multiply_reduce_fusion
  663.3 7.3 %copy.54 = bf16[8,2048,256]{2,1,0:T(8,128)(2,1)} copy(bf16[8,2048,256]{2,1,0:T(8,128)(2,1)} %all-gather.4.cloned.1.call-done) | data formatting | bytes 16777216
  670.6 7.3 %copy.55 = bf16[8,2048,256]{2,1,0:T(8,128)(2,1)} copy(bf16[8,2048,256]{2,1,0:T(8,128)(2,1)} %all-gather.6.cloned.1.call-done) | data formatting | bytes 16777216
  677.9 7.3 %copy.56 = bf16[8,2048,256]{2,1,0:T(8,128)(2,1)} copy(bf16[8,2048,256]{2,1,0:T(8,128)(2,1)} %all-gather.8.cloned.1.call-done) | data formatting | bytes 16777216
  (34 shorter events, 1.5 us)
Async XLA Ops:
  119.2 97.8 %all-to-all-start = ((bf16[32,256,256]{2,1,0:T(8,128)(2,1)}), bf16[32,256,256]{2,1,0:T(8,128)(2,1)}, u32[]{:S(2)}, u32[]{:S(2)}) async-start(bf16[32,256,256]{2,1,0:T(8,128)(2,1)} %get-tuple-element.5), calls=%async_computation | async-start | bytes 8388608 | tf_op jit(solution)/shard_map/all_to_all | solution.py:19
  124.1 378.8 %all-gather.6.cloned.1.call-start = ((), (), s32[]{:S(2)}) async-start(), calls=%async_computation.7 | async-start | bytes 12582912 | tf_op jit(solution)/shard_map/all_gather | solution.py:25
  217.0 97.6 %all-to-all-start.2 = ((bf16[32,256,256]{2,1,0:T(8,128)(2,1)}), bf16[32,256,256]{2,1,0:T(8,128)(2,1)}, u32[]{:S(2)}, u32[]{:S(2)}) async-start(bf16[32,256,256]{2,1,0:T(8,128)(2,1)} %convert_element_type.42), calls=%async_computation.2 | async-start | bytes 8388608 | tf_op jit(solution)/shard_map/all_to_all | solution.py:21
  221.9 289.2 %all-gather.4.cloned.1.call-start = ((), (), s32[]{:S(2)}) async-start(), calls=%async_computation.6 | async-start | bytes 12582912 | tf_op jit(solution)/shard_map/all_gather | solution.py:24
  226.6 0.7 copy-start.1
  226.6 15.4 %copy-start = (bf16[512,2048]{1,0:T(8,128)(2,1)S(1)}, bf16[512,2048]{1,0:T(8,128)(2,1)}, u32[]{:S(2)}) copy-start(bf16[512,2048]{1,0:T(8,128)(2,1)} %param.7) | copy-start | bytes 6291460
  314.6 188.3 %all-to-all-start.3 = ((bf16[4,8,64,2048]{3,2,1,0:T(8,128)(2,1)}), bf16[4,8,64,2048]{3,2,1,0:T(8,128)(2,1)}, u32[]{:S(2)}, u32[]{:S(2)}) async-start(bf16[4,8,64,2048]{3,2,1,0:T(8,128)(2,1)} %bitcast.75), calls=%async_computation.3 | async-start | bytes 16777216 | tf_op jit(solution)/shard_map/all_to_all | solution.py:43
  320.3 190.8 %all-gather.8.cloned.1.call-start = ((), (), s32[]{:S(2)}) async-start(), calls=%async_computation.8 | async-start | bytes 12582912 | tf_op jit(solution)/shard_map/all_gather | solution.py:26
  325.1 273.1 %reduce-scatter.2.cloned.1.call-start = ((), (), s32[]{:S(2)}) async-start(), calls=%async_computation.9 | async-start | bytes 10485760 | tf_op jit(solution)/shard_map/reduce_scatter | solution.py:55
  528.2 77.8 %copy-start.2 = (f32[512,2]{0,1:T(2,128)S(1)}, f32[512,2]{0,1:T(2,128)}, u32[]{:S(2)}) copy-start(f32[512,2]{0,1:T(2,128)} %param.13) | copy-start | bytes 12292
  601.3 52.6 %all-to-all-start.4 = ((bf16[4,8,64,512]{3,2,1,0:T(8,128)(2,1)}), bf16[4,8,64,512]{3,2,1,0:T(8,128)(2,1)S(1)}, u32[]{:S(2)}, u32[]{:S(2)}) async-start(bf16[4,8,64,512]{3,2,1,0:T(8,128)(2,1)} %copy.36), calls=%async_computation.5 | async-start | bytes 4194304 | tf_op jit(solution)/shard_map/all_to_all | solution.py:58
Sparse Core Ops, SparseCore 0:
  129.0 105.3 all-gather.5
  236.5 103.9 all-gather.3
  342.1 103.9 all-gather.7
  528.3 69.8 reduce-scatter.1
where the time goes:
time: 693 us; the launch traced here: 692 us
  waiting for transfers between devices  437 us (63%)
  blocking collectives  101 us (15%)
  local copies, waits for them, and re-layouts  61.4 us (9%)
  other arithmetic  33.5 us (5%)
  matrix products  25.1 us (4%)
  starting transfers between devices  20.4 us (3%)
  between operations  14 us (2%)
    all_to_all x1, waiting for transfers between devices, per_device(): lax.all_to_all(outgoing, 'fs', split_axis=0, concat_axis=0, tiled=True)  178 us
    all_to_all x1, blocking collectives, per_device(): lax.all_to_all(up_low, 'fs', split_axis=0, concat_axis=1, tiled=True)  101 us
    all_to_all x1, waiting for transfers between devices, per_device(): lax.all_to_all(gate_low, 'fs', split_axis=0, concat_axis=1, tiled=True)  82.3 us
    reduce_scatter x1, waiting for transfers between devices, per_device(): lax.psum_scatter(partial_value, 'tp', scatter_dimension=3, tiled=True)  70 us
    all_to_all x1, waiting for transfers between devices, per_device(): lax.all_to_all(down_low, 'fs', split_axis=0, concat_axis=1, tiled=True)  58.9 us
    all_to_all x1, waiting for transfers between devices, per_device(): lax.all_to_all(summed.astype(jnp.bfloat16), 'fs', split_axis=0, concat_ax...  47.9 us
    unnamed x11, local copies, waits for them, and re-layouts  22.9 us
    dot_general x1, matrix products, per_device(): jnp.einsum('secf,edf->secd', hidden, down_ready, preferred_element_type=j...  17 us
  transfers between devices with their start and end apart: 8, of which 5 were waited for; matrix products, arithmetic and copies ran while one was open for 8% of the time, Pallas kernels for 0%

commit v1 on v0

--- a/solution.py
+++ b/solution.py
@@ -17,7 +17,10 @@
     local_experts = experts // fs_count
     resharded = (
         lax.all_to_all(gate_low, "fs", split_axis=0, concat_axis=1, tiled=True),
-        lax.all_to_all(up_low, "fs", split_axis=0, concat_axis=1, tiled=True),
+        jnp.concatenate(
+            lax.all_to_all(jnp.stack(jnp.split(up_low, lax.axis_size("fs"), axis=0)), "fs", 0, 0),
+            axis=1,
+        ),
         lax.all_to_all(down_low, "fs", split_axis=0, concat_axis=1, tiled=True),
     )
     gate_ready, up_ready, down_ready = (

time: 693 us -> 695 us (level)
  no operation moved by 1% of the time
where the time goes in v1:
time: 695 us; the launch traced here: 694 us
  waiting for transfers between devices  437 us (63%)
  blocking collectives  99.4 us (14%)
  local copies, waits for them, and re-layouts  64 us (9%)
  other arithmetic  34.1 us (5%)
  matrix products  25.1 us (4%)
  starting transfers between devices  20.4 us (3%)
  between operations  14 us (2%)
    all_to_all x1, waiting for transfers between devices, per_device(): lax.all_to_all(outgoing, 'fs', split_axis=0, concat_axis=0, tiled=True)  178 us
    all_to_all x1, blocking collectives, per_device(): lax.all_to_all(jnp.stack(jnp.split(up_low, lax.axis_size('fs'), axis=0)),...  99.4 us
    all_to_all x1, waiting for transfers between devices, per_device(): lax.all_to_all(gate_low, 'fs', split_axis=0, concat_axis=1, tiled=True)  81.8 us
    reduce_scatter x1, waiting for transfers between devices, per_device(): lax.psum_scatter(partial_value, 'tp', scatter_dimension=3, tiled=True)  70.4 us
    all_to_all x1, waiting for transfers between devices, per_device(): lax.all_to_all(down_low, 'fs', split_axis=0, concat_axis=1, tiled=True)  58.9 us
    all_to_all x1, waiting for transfers between devices, per_device(): lax.all_to_all(summed.astype(jnp.bfloat16), 'fs', split_axis=0, concat_ax...  47.8 us
    unnamed x11, local copies, waits for them, and re-layouts  22.9 us
    dot_general x1, matrix products, per_device(): jnp.einsum('secf,edf->secd', hidden, down_ready, preferred_element_type=j...  17 us
  transfers between devices with their start and end apart: 8, of which 5 were waited for; matrix products, arithmetic and copies ran while one was open for 8% of the time, Pallas kernels for 0%

profile of v1, /device:TPU:0, one launch (start us, length us, event | category | flops | bytes accessed | tf_op | source)
XLA Modules:
  0.0 693.7 jit_solution(2288694139463486758)
XLA Ops:
  7.2 11.5 %multiply_convert_fusion.1 = (bf16[32,256,256]{2,1,0:T(8,128)(2,1)}, bf16[32,256,256]{2,1,0:T(8,128)(2,1)}) fusion(f32[32,256,256]{2,1,0:T(8,128)} %param.10, f32[256]{0:T(256)} %param.8, f32[32,256,256]{2,1,0:T(8,128)} %param.9), kind=kLoop, calls=%fused_computation.11 | loop fusion | flops 8388608 | bytes 25166848 | tf_op jit(solution)/shard_map/convert_element_type | solution.py:13
  18.7 2.6 slice_bitcast_fusion.3
  21.3 0.6 pad_maximum_fusion
  21.9 99.4 %all_to_all.51 = bf16[4,8,256,256]{3,2,1,0:T(8,128)(2,1)} all-to-all(bf16[4,8,256,256]{3,2,1,0:T(8,128)(2,1)S(1)} %pad_maximum_fusion), channel_id=1, replica_groups=mesh['gr'=2,'fs'=4,'tp'=4] {'fs'}, dimensions={0} | all-to-all | bytes 8388608 | tf_op jit(solution)/shard_map/all_to_all | solution.py:21
  121.2 4.9 all-to-all-start
  126.2 4.6 copy.27
  130.9 5.9 convert_element_type.42
  136.8 81.8 %all-to-all-done = bf16[32,256,256]{2,1,0:T(8,128)(2,1)} async-done(((bf16[32,256,256]{2,1,0:T(8,128)(2,1)}), bf16[32,256,256]{2,1,0:T(8,128)(2,1)}, u32[]{:S(2)}, u32[]{:S(2)}) %all-to-all-start) | async-done | bytes 4194336 | tf_op jit(solution)/shard_map/all_to_all | solution.py:19
  218.6 4.8 all-to-all-start.2
  223.5 4.6 copy.26
  228.1 0.7 copy-done.1
  229.3 9.0 %reduce-window.6 = s32[32,8,128]{2,1,0:T(8,128)S(1)} reduce-window(s32[32,8,128]{2,1,0:T(8,128)S(1)} %fusion.29, s32[]{:T(128)} %constant.36.clone.1), window={size=1x1x128 pad=0_0x0_0x127_0}, to_apply=%region_1.0 | reduce-window | flops 4161536 | bytes 262148 | tf_op jit(solution)/shard_map/reduce-window
  239.2 4.3 scatter_custom_fusion
  243.5 0.5 fusion.9
  244.0 2.3 fusion.10
  246.4 10.9 %gather_fusion = bf16[2048,2048]{1,0:T(8,128)(2,1)} fusion(bf16[512,2048]{1,0:T(8,128)(2,1)S(1)} %fusion.10, s32[2048]{0:T(1024)S(1)} %fusion.30), kind=kCustom, calls=%fused_computation | custom fusion | bytes 16785408 | tf_op jit(solution)/shard_map/gather | solution.py:45
  257.2 58.9 %all-to-all-done.2 = bf16[32,256,256]{2,1,0:T(8,128)(2,1)} async-done(((bf16[32,256,256]{2,1,0:T(8,128)(2,1)}), bf16[32,256,256]{2,1,0:T(8,128)(2,1)}, u32[]{:S(2)}, u32[]{:S(2)}) %all-to-all-start.2) | async-done | bytes 4194336 | tf_op jit(solution)/shard_map/all_to_all | solution.py:24
  316.2 5.7 all-to-all-start.3
  321.9 4.7 copy.28
  326.8 177.7 %all-to-all-done.3 = bf16[4,8,64,2048]{3,2,1,0:T(8,128)(2,1)} async-done(((bf16[4,8,64,2048]{3,2,1,0:T(8,128)(2,1)}), bf16[4,8,64,2048]{3,2,1,0:T(8,128)(2,1)}, u32[]{:S(2)}, u32[]{:S(2)}) %all-to-all-start.3) | async-done | bytes 8388640 | tf_op jit(solution)/shard_map/all_to_all | solution.py:46
  504.5 8.1 %fusion.3 = f32[8,256,4,64]{1,3,2,0:T(8,128)S(1)} fusion(bf16[8,2048,256]{2,1,0:T(8,128)(2,1)} %all-gather.6.cloned.1.call-done, bf16[4,8,64,2048]{3,2,1,0:T(8,128)(2,1)} %all-to-all-done.3), kind=kOutput, calls=%fused_computation.7 | convolution fusion | flops 2147483648 | bytes 18874368 | tf_op jit(solution)/shard_map/secd,edf->secf/dot_general | solution.py:50
  512.6 17.0 %fusion = bf16[4,8,64,2048]{3,2,0,1:T(8,128)(2,1)} fusion(bf16[8,2048,256]{2,1,0:T(8,128)(2,1)} %all-gather.8.cloned.1.call-done, f32[8,256,4,64]{1,3,2,0:T(8,128)S(1)} %fusion.3, bf16[4,8,64,2048]{3,2,1,0:T(8,128)(2,1)} %all-to-all-done.3, bf16[8,2048,256]{2,1,0:T(8,128)(2,1)} %all-gather.4.cloned.1.call-done), kind=kOutput, calls=%fused_computation.4 | convolution fusion | flops 4307550208 | bytes 35651584 | tf_op jit(solution)/shard_map/secf,edf->secd/dot_general | solution.py:55
  529.7 70.4 %reduce-scatter.2.cloned.1.call-done = bf16[4,8,64,512]{3,2,0,1:T(8,128)(2,1)} async-done(((bf16[4,8,64,2048]{3,2,0,1:T(8,128)(2,1)}), bf16[4,8,64,512]{3,2,0,1:T(8,128)(2,1)}) %reduce-scatter.2.cloned.1.call-update) | async-done | bytes 2097168 | tf_op jit(solution)/shard_map/reduce_scatter | solution.py:58
  600.2 3.1 copy.36
  603.3 4.6 all-to-all-start.4
  608.1 47.8 %all-to-all-done.4 = bf16[4,8,64,512]{3,2,1,0:T(8,128)(2,1)S(1)} async-done(((bf16[4,8,64,512]{3,2,1,0:T(8,128)(2,1)}), bf16[4,8,64,512]{3,2,1,0:T(8,128)(2,1)S(1)}, u32[]{:S(2)}, u32[]{:S(2)}) %all-to-all-start.4) | async-done | bytes 2097184 | tf_op jit(solution)/shard_map/all_to_all | solution.py:61
  655.9 4.0 gather_fusion.1
  659.9 1.3 reshape.86
  661.2 4.0 multiply_reduce_fusion
  665.3 7.3 %copy.54 = bf16[8,2048,256]{2,1,0:T(8,128)(2,1)} copy(bf16[8,2048,256]{2,1,0:T(8,128)(2,1)} %all-gather.4.cloned.1.call-done) | data formatting | bytes 16777216
  672.6 7.3 %copy.55 = bf16[8,2048,256]{2,1,0:T(8,128)(2,1)} copy(bf16[8,2048,256]{2,1,0:T(8,128)(2,1)} %all-gather.6.cloned.1.call-done) | data formatting | bytes 16777216
  679.9 7.3 %copy.56 = bf16[8,2048,256]{2,1,0:T(8,128)(2,1)} copy(bf16[8,2048,256]{2,1,0:T(8,128)(2,1)} %all-gather.8.cloned.1.call-done) | data formatting | bytes 16777216
  (36 shorter events, 1.9 us)
Async XLA Ops:
  121.2 97.3 %all-to-all-start = ((bf16[32,256,256]{2,1,0:T(8,128)(2,1)}), bf16[32,256,256]{2,1,0:T(8,128)(2,1)}, u32[]{:S(2)}, u32[]{:S(2)}) async-start(bf16[32,256,256]{2,1,0:T(8,128)(2,1)} %get-tuple-element.9), calls=%async_computation | async-start | bytes 8388608 | tf_op jit(solution)/shard_map/all_to_all | solution.py:19
  126.2 378.3 %all-gather.6.cloned.1.call-start = ((), (), s32[]{:S(2)}) async-start(), calls=%async_computation.7 | async-start | bytes 12582912 | tf_op jit(solution)/shard_map/all_gather | solution.py:28
  218.6 97.6 %all-to-all-start.2 = ((bf16[32,256,256]{2,1,0:T(8,128)(2,1)}), bf16[32,256,256]{2,1,0:T(8,128)(2,1)}, u32[]{:S(2)}, u32[]{:S(2)}) async-start(bf16[32,256,256]{2,1,0:T(8,128)(2,1)} %convert_element_type.42), calls=%async_computation.2 | async-start | bytes 8388608 | tf_op jit(solution)/shard_map/all_to_all | solution.py:24
  223.4 289.2 %all-gather.4.cloned.1.call-start = ((), (), s32[]{:S(2)}) async-start(), calls=%async_computation.6 | async-start | bytes 12582912 | tf_op jit(solution)/shard_map/all_gather | solution.py:27
  228.1 0.7 copy-start.1
  228.1 15.4 %copy-start = (bf16[512,2048]{1,0:T(8,128)(2,1)S(1)}, bf16[512,2048]{1,0:T(8,128)(2,1)}, u32[]{:S(2)}) copy-start(bf16[512,2048]{1,0:T(8,128)(2,1)} %param.7) | copy-start | bytes 6291460
  316.2 188.3 %all-to-all-start.3 = ((bf16[4,8,64,2048]{3,2,1,0:T(8,128)(2,1)}), bf16[4,8,64,2048]{3,2,1,0:T(8,128)(2,1)}, u32[]{:S(2)}, u32[]{:S(2)}) async-start(bf16[4,8,64,2048]{3,2,1,0:T(8,128)(2,1)} %bitcast.81), calls=%async_computation.3 | async-start | bytes 16777216 | tf_op jit(solution)/shard_map/all_to_all | solution.py:46
  321.8 190.8 %all-gather.8.cloned.1.call-start = ((), (), s32[]{:S(2)}) async-start(), calls=%async_computation.8 | async-start | bytes 12582912 | tf_op jit(solution)/shard_map/all_gather | solution.py:29
  326.6 273.6 %reduce-scatter.2.cloned.1.call-start = ((), (), s32[]{:S(2)}) async-start(), calls=%async_computation.9 | async-start | bytes 10485760 | tf_op jit(solution)/shard_map/reduce_scatter | solution.py:58
  529.7 78.2 %copy-start.2 = (f32[512,2]{0,1:T(2,128)S(1)}, f32[512,2]{0,1:T(2,128)}, u32[]{:S(2)}) copy-start(f32[512,2]{0,1:T(2,128)} %param.13) | copy-start | bytes 12292
  603.3 52.6 %all-to-all-start.4 = ((bf16[4,8,64,512]{3,2,1,0:T(8,128)(2,1)}), bf16[4,8,64,512]{3,2,1,0:T(8,128)(2,1)S(1)}, u32[]{:S(2)}, u32[]{:S(2)}) async-start(bf16[4,8,64,512]{3,2,1,0:T(8,128)(2,1)} %copy.36), calls=%async_computation.5 | async-start | bytes 4194304 | tf_op jit(solution)/shard_map/all_to_all | solution.py:61
Sparse Core Ops, SparseCore 0:
  131.0 105.3 all-gather.5
  238.5 103.9 all-gather.3
  344.1 103.9 all-gather.7
  529.8 70.2 reduce-scatter.1
